TPU v7x, 32 devices: a whole 2x2x4 slice. The times are simulated.
32 devices in a mesh: grp: 2 (over x), ep: 16 (over z, y, core), tp: 1.
Axes of the slice: x: 2, y: 2, z: 4, core: 2. Of those that a mesh axis runs over, the one named last changes fastest.
Arguments:
- tokens: bfloat16 [2048, 1024], P(('grp', 'ep')), parts along dimension 0, may hold values from -6 to 6
- norm_gain: float32 [1024], replicated, may hold values from 0.1 to 1.9
- routes: int32 [2048, 6], P(('grp', 'ep')), parts along dimension 0, may hold values from 0 to 15, all different within a row; in each aligned block of 64 rows (0 to 63, 64 to 127, ...) at most 32 rows name the same one
- gate_weights: float32 [2048, 6], P(('grp', 'ep')), parts along dimension 0, may hold values from 0.1 to 1
- w_gate: bfloat16 [16, 1024, 2048], P('ep', None, 'tp'), may hold values from -0.1875 to 0.1875
- w_up: bfloat16 [16, 1024, 2048], P('ep', None, 'tp'), may hold values from -0.1875 to 0.1875
- w_down: bfloat16 [16, 2048, 1024], P('ep', 'tp'), may hold values from -0.125 to 0.125
Outputs:
- mixed: bfloat16 [2048, 1024], P(('grp', 'ep')), parts along dimension 0
There are 2 independent parts, one for each index of `grp`. A program takes and returns all parts, laid end to end along the dimension named above; an argument that names none is the same for every part. Nothing has to cross between parts.
Inputs may be any that keep to these rules, and one draw needn't show every extreme that they name: `routes`: each row names 6 different experts. Within the rows of one index of ep no expert is named more than 32 times, and in every draw some expert is named exactly 32 times in some index's rows.
All inputs are finite; a program needn't handle non-finite values.
Results may differ from a plain program's by a relative error of at most 0.013.
Values may be sent and summed in bfloat16 or wider, within the bound.
No kernel may reach another device: no remote copies, remote signals or barrier semaphores. Data moves between devices by JAX's collectives and lax.ppermute only.
A program may use at most 64 MiB of HBM per device.

v0:
```python
import jax
import jax.numpy as jnp
from jax import lax
from jax.sharding import PartitionSpec as P


def hidden_rows(rows, w_gate, w_up):
    gate = jnp.dot(rows, w_gate[0], preferred_element_type=jnp.float32)
    up = jnp.dot(rows, w_up[0], preferred_element_type=jnp.float32)
    return (jax.nn.silu(gate) * up).astype(jnp.bfloat16)


def weigh_rows(combine, returned):
    upper = combine.astype(jnp.bfloat16)
    lower = (combine - upper.astype(jnp.float32)).astype(jnp.bfloat16)
    first = jnp.dot(upper, returned, preferred_element_type=jnp.float32)
    return first + jnp.dot(lower, returned, preferred_element_type=jnp.float32)


def shards(tokens, norm_gain, routes, gate_weights, w_gate, w_up, w_down):
    values = tokens.astype(jnp.float32)
    scale = lax.rsqrt(jnp.mean(values * values, axis=-1, keepdims=True) + 1e-06)
    normed = (values * scale * norm_gain).astype(jnp.bfloat16)
    width = tokens.shape[1]
    tok_dev = tokens.shape[0]
    topk = routes.shape[1]
    experts = lax.axis_size("ep")
    capacity = min(tok_dev, max(2, 4 * tok_dev * topk // (3 * experts)))
    expert_ids = jnp.arange(experts, dtype=jnp.int32)
    hits = routes[:, :, None] == expert_ids[None, None, :]
    chosen = jnp.any(hits, axis=1).astype(jnp.int32)
    weight_tok = jnp.sum(jnp.where(hits, gate_weights[:, :, None], 0.0), axis=1)
    rank = jnp.cumsum(chosen, axis=0) - chosen
    slot = jnp.where(chosen > 0, rank * experts + expert_ids[None, :], -1)
    slot_ids = jnp.arange(capacity * experts, dtype=jnp.int32)
    placed = slot[:, :, None] == slot_ids[None, None, :]
    place = jnp.any(placed, axis=1).astype(jnp.bfloat16)
    combine = jnp.sum(jnp.where(placed, weight_tok[:, :, None], 0.0), axis=1)
    dispatch = jnp.dot(place.T, normed, preferred_element_type=jnp.float32)
    dispatch = dispatch.astype(jnp.bfloat16).reshape(capacity, experts, width)
    arrived = lax.all_to_all(dispatch, "ep", split_axis=1, concat_axis=1, tiled=True)
    rows = arrived.reshape(-1, width)
    partial_value = jnp.dot(
        hidden_rows(rows, w_gate, w_up), w_down[0], preferred_element_type=jnp.float32
    )
    output = lax.psum(partial_value.astype(jnp.bfloat16), "tp")
    returned = lax.all_to_all(
        output.reshape(arrived.shape), "ep", split_axis=1, concat_axis=1, tiled=True
    )
    mixed = weigh_rows(combine, returned.reshape(-1, width))
    return mixed.astype(jnp.bfloat16)


def solution(mesh):
    in_specs = (
        P(("grp", "ep"), None),
        P(),
        P(("grp", "ep"), None),
        P(("grp", "ep"), None),
        P("ep", None, "tp"),
        P("ep", None, "tp"),
        P("ep", "tp", None),
    )
    out_specs = P(("grp", "ep"), None)
    return jax.shard_map(shards, mesh=mesh, in_specs=in_specs, out_specs=out_specs, check_vma=False)
```

profile of v0, /device:TPU:11, one launch (start us, length us, event | category | flops | bytes accessed | tf_op | source)
XLA Modules:
  0.0 83.4 jit_solution(14729144316334113847)
XLA Ops:
  0.0 0.7 fusion.23
  0.7 0.1 copy.20
  0.8 0.1 reduce_window_sum.11
  0.9 0.0 copy-start.2
  0.9 0.5 fusion.8
  1.5 1.3 %fusion.17 = f32[64]{0:T(128)S(1)} fusion(bf16[64,1024]{1,0:T(8,128)(2,1)} %param.7), kind=kLoop, calls=%fused_computation.16 | loop fusion | flops 196544 | bytes 131328 | tf_op jit(solution)/shard_map/reduce_sum | solution.py:22
  2.8 1.4 %convolution_convert_fusion = bf16[512,1024]{1,0:T(8,128)(2,1)S(1)} fusion(pred[64,512]{1,0:T(8,128)(4,1)S(1)} %fusion.8, bf16[64,1024]{1,0:T(8,128)(2,1)} %param.7, f32[1024]{0:T(1024)} %param.8, f32[64]{0:T(128)S(1)} %add_rsqrt_fusion), kind=kOutput, calls=%fused_computation.10 | convolution fusion | flops 67895296 | bytes 1216768 | tf_op jit(solution)/shard_map/dot_general | solution.py:39
  4.2 0.6 copy.22
  4.8 31.7 %all_to_all.10 = bf16[32,16,1024]{2,0,1:T(8,128)(2,1)S(1)} all-to-all(bf16[32,16,1024]{2,0,1:T(8,128)(2,1)S(1)} %copy.22), channel_id=1, replica_groups=mesh['grp'=2,'ep'=16,'tp'=1] {'ep'}, dimensions={1} | all-to-all | bytes 2097152 | tf_op jit(solution)/shard_map/all_to_all | solution.py:41
  36.5 0.6 copy.23
  37.1 0.0 copy-done.2
  37.1 4.3 %fusion.4 = f32[512,2048]{1,0:T(8,128)} fusion(bf16[512,1024]{1,0:T(8,128)(2,1)S(1)} %bitcast.29, bf16[1,1024,2048]{2,1,0:T(8,128)(2,1)S(1)} %copy-done.2), kind=kOutput, calls=%fused_computation.4 | convolution fusion | flops 2147483648 | bytes 9437184 | tf_op jit(solution)/shard_map/dot_general | solution.py:8
  41.4 9.2 %fusion.11 = bf16[512,1024]{1,0:T(8,128)(2,1)S(1)} fusion(bf16[1,2048,1024]{2,1,0:T(8,128)(2,1)} %param.13, f32[512,2048]{1,0:T(8,128)} %fusion.4, bf16[512,1024]{1,0:T(8,128)(2,1)S(1)} %bitcast.30, bf16[1,1024,2048]{2,1,0:T(8,128)(2,1)} %param.12), kind=kOutput, calls=%fused_computation.11 | convolution fusion | flops 4301783040 | bytes 14680064 | tf_op jit(solution)/shard_map/dot_general | solution.py:43
  50.6 0.0 copy-start
  50.6 0.0 copy-start.1
  50.7 1.6 %copy.24 = bf16[32,16,1024]{2,0,1:T(8,128)(2,1)} copy(bf16[32,16,1024]{2,1,0:T(8,128)(2,1)S(1)} %bitcast.31) | data formatting | bytes 2097152 | tf_op jit(solution)/shard_map/reshape | solution.py:48
  52.2 4.4 %all-to-all-start.1 = ((bf16[32,16,1024]{2,0,1:T(8,128)(2,1)}), bf16[32,16,1024]{2,0,1:T(8,128)(2,1)S(1)}, u32[]{:S(2)}, u32[]{:S(2)}) async-start(bf16[32,16,1024]{2,0,1:T(8,128)(2,1)} %copy.24), calls=%async_computation.1 | async-start | bytes 2097152 | tf_op jit(solution)/shard_map/all_to_all | solution.py:47
  56.6 0.0 copy-done
  56.6 0.0 copy-done.1
  56.7 0.1 copy.21
  56.7 0.6 select_reduce_fusion
  57.4 24.2 %all-to-all-done.1 = bf16[32,16,1024]{2,0,1:T(8,128)(2,1)S(1)} async-done(((bf16[32,16,1024]{2,0,1:T(8,128)(2,1)}), bf16[32,16,1024]{2,0,1:T(8,128)(2,1)S(1)}, u32[]{:S(2)}, u32[]{:S(2)}) %all-to-all-start.1) | async-done | bytes 1048608 | tf_op jit(solution)/shard_map/all_to_all | solution.py:47
  81.5 0.6 copy.25
  82.1 0.3 fusion.25
  82.4 1.0 %fusion.16 = bf16[64,1024]{1,0:T(8,128)(2,1)} fusion(f32[64,1024]{1,0:T(8,128)S(1)} %fusion.25, bf16[512,1024]{1,0:T(8,128)(2,1)S(1)} %bitcast.27, f32[64,512]{1,0:T(8,128)S(1)} %select_reduce_fusion), kind=kOutput, calls=%fused_computation.13 | convolution fusion | flops 67371008 | bytes 1572864 | tf_op jit(solution)/shard_map/dot_general | solution.py:17
  (4 shorter events, 0.0 us)
Async XLA Ops:
  0.9 36.2 %copy-start.2 = (bf16[1,1024,2048]{2,1,0:T(8,128)(2,1)S(1)}, bf16[1,1024,2048]{2,1,0:T(8,128)(2,1)}, u32[]{:S(2)}) copy-start(bf16[1,1024,2048]{2,1,0:T(8,128)(2,1)} %param.11) | copy-start | bytes 12582916
  50.6 6.0 %copy-start = (s32[64,6]{0,1:T(8,128)S(1)}, s32[64,6]{0,1:T(8,128)}, u32[]{:S(2)}) copy-start(s32[64,6]{0,1:T(8,128)} %param.9) | copy-start | bytes 4612
  50.6 6.0 %copy-start.1 = (f32[64,6]{0,1:T(8,128)S(1)}, f32[64,6]{0,1:T(8,128)}, u32[]{:S(2)}) copy-start(f32[64,6]{0,1:T(8,128)} %param.10) | copy-start | bytes 4612
  52.2 29.3 %all-to-all-start.1 = ((bf16[32,16,1024]{2,0,1:T(8,128)(2,1)}), bf16[32,16,1024]{2,0,1:T(8,128)(2,1)S(1)}, u32[]{:S(2)}, u32[]{:S(2)}) async-start(bf16[32,16,1024]{2,0,1:T(8,128)(2,1)} %copy.24), calls=%async_computation.1 | async-start | bytes 2097152 | tf_op jit(solution)/shard_map/all_to_all | solution.py:47
where the time goes:
time: 83.7 us; the launch traced here: 83.4 us
  blocking collectives  31.7 us (38%)
  waiting for transfers between devices  24.2 us (29%)
  matrix products  16.2 us (19%)
  starting transfers between devices  4.39 us (5%)
  local copies, waits for them, and re-layouts  3.51 us (4%)
  other arithmetic  3.31 us (4%)
    all_to_all x1, blocking collectives, shards(): lax.all_to_all(dispatch, 'ep', split_axis=1, concat_axis=1, tiled=True)  31.7 us
    all_to_all x1, waiting for transfers between devices, shards(): lax.all_to_all(output.reshape(arrived.shape), 'ep', split_axis=1, concat_...  24.2 us
    dot_general x1, matrix products, shards(): jnp.dot(hidden_rows(rows, w_gate, w_up), w_down[0], preferred_element_typ...  9.21 us
    all_to_all x1, starting transfers between devices, shards(): lax.all_to_all(output.reshape(arrived.shape), 'ep', split_axis=1, concat_...  4.39 us
    dot_general x1, matrix products, hidden_rows(): gate = jnp.dot(rows, w_gate[0], preferred_element_type=jnp.float32)  4.29 us
  transfers between devices with their start and end apart: 1, of which 1 were waited for; matrix products, arithmetic and copies ran while one was open for 1% of the time, Pallas kernels for 0%

commit v1 on v0

--- a/solution.py
+++ b/solution.py
@@ -44,9 +44,19 @@
         hidden_rows(rows, w_gate, w_up), w_down[0], preferred_element_type=jnp.float32
     )
     output = lax.psum(partial_value.astype(jnp.bfloat16), "tp")
-    returned = lax.all_to_all(
-        output.reshape(arrived.shape), "ep", split_axis=1, concat_axis=1, tiled=True
-    )
+    x = output.reshape(arrived.shape)
+    ways, here = (lax.axis_size("ep"), lax.axis_index("ep"))
+    width_2 = x.shape[1] // ways
+    shape = list(x.shape)
+    shape[1] = width_2
+    height = shape[1]
+    shape[1] = height * ways
+    returned = jnp.zeros(shape, x.dtype)
+    for mask in range(ways):
+        part = lax.dynamic_slice_in_dim(x, (here ^ mask) * width_2, width_2, axis=1)
+        if mask:
+            part = lax.ppermute(part, "ep", [(d, d ^ mask) for d in range(ways)])
+        returned = lax.dynamic_update_slice_in_dim(returned, part, (here ^ mask) * height, axis=1)
     mixed = weigh_rows(combine, returned.reshape(-1, width))
     return mixed.astype(jnp.bfloat16)
 

time: 83.7 us -> 122 us (1.46)
  the two profiles are of different devices: /device:TPU:11 before, /device:TPU:7 now
where the time goes in v1:
time: 122 us; the launch traced here: 121 us
  waiting for transfers between devices  41 us (34%)
  starting transfers between devices  32.5 us (27%)
  local copies, waits for them, and re-layouts  26.3 us (22%)
  matrix products  18.4 us (15%)
  other arithmetic  3.04 us (2%)
    ppermute x15, starting transfers between devices, shards(): part = lax.ppermute(part, 'ep', [(d, d ^ mask) for d in range(ways)])  25.9 us
    all_to_all x1, waiting for transfers between devices, shards(): lax.all_to_all(dispatch, 'ep', split_axis=1, concat_axis=1, tiled=True)  23.5 us
    dynamic_update_slice x16, local copies, waits for them, and re-layouts, shards(): lax.dynamic_update_slice_in_dim(returned, part, (here ^ mask) * height, a...  21 us
    ppermute x15, waiting for transfers between devices, shards(): part = lax.ppermute(part, 'ep', [(d, d ^ mask) for d in range(ways)])  17.4 us
    dot_general x1, matrix products, shards(): jnp.dot(hidden_rows(rows, w_gate, w_up), w_down[0], preferred_element_typ...  9.22 us
    all_to_all x1, starting transfers between devices, shards(): lax.all_to_all(dispatch, 'ep', split_axis=1, concat_axis=1, tiled=True)  6.63 us
    dot_general x1, matrix products, hidden_rows(): gate = jnp.dot(rows, w_gate[0], preferred_element_type=jnp.float32)  6.46 us
    dynamic_slice x1, local copies, waits for them, and re-layouts, shards(): part = lax.dynamic_slice_in_dim(x, (here ^ mask) * width_2, width_2, axis=1)  2.78 us
  transfers between devices with their start and end apart: 16, of which 6 were waited for; matrix products, arithmetic and copies ran while one was open for 17% of the time, Pallas kernels for 0%

profile of v1, /device:TPU:7, one launch (start us, length us, event | category | flops | bytes accessed | tf_op | source)
XLA Modules:
  0.0 121.4 jit_solution(3952338239339115520)
XLA Ops:
  0.0 0.7 fusion.24
  0.7 0.1 copy.17
  0.8 0.1 reduce_window_sum.11
  0.9 0.5 fusion.8
  1.5 1.0 fusion.17
  2.5 1.4 %convolution_convert_fusion = bf16[512,1024]{1,0:T(8,128)(2,1)S(1)} fusion(pred[64,512]{1,0:T(8,128)(4,1)S(1)} %fusion.8, bf16[64,1024]{1,0:T(8,128)(2,1)} %param.7, f32[1024]{0:T(1024)} %param.8, f32[64]{0:T(128)S(1)} %add_rsqrt_fusion), kind=kOutput, calls=%fused_computation.10 | convolution fusion | flops 67895296 | bytes 1216768 | tf_op jit(solution)/shard_map/dot_general | solution.py:39
  3.9 1.6 %copy.19 = bf16[32,16,1024]{2,0,1:T(8,128)(2,1)} copy(bf16[32,16,1024]{2,1,0:T(8,128)(2,1)S(1)} %bitcast.29) | data formatting | bytes 2097152 | tf_op jit(solution)/shard_map/reshape | solution.py:40
  5.5 6.6 %all-to-all-start = ((bf16[32,16,1024]{2,0,1:T(8,128)(2,1)}), bf16[32,16,1024]{2,0,1:T(8,128)(2,1)S(1)}, u32[]{:S(2)}, u32[]{:S(2)}) async-start(bf16[32,16,1024]{2,0,1:T(8,128)(2,1)} %copy.19), calls=%async_computation | async-start | bytes 2097152 | tf_op jit(solution)/shard_map/all_to_all | solution.py:41
  12.1 23.5 %all-to-all-done = bf16[32,16,1024]{2,0,1:T(8,128)(2,1)S(1)} async-done(((bf16[32,16,1024]{2,0,1:T(8,128)(2,1)}), bf16[32,16,1024]{2,0,1:T(8,128)(2,1)S(1)}, u32[]{:S(2)}, u32[]{:S(2)}) %all-to-all-start) | async-done | bytes 1048608 | tf_op jit(solution)/shard_map/all_to_all | solution.py:41
  35.6 0.6 copy.20
  36.2 6.5 %fusion.4 = f32[512,2048]{1,0:T(8,128)} fusion(bf16[512,1024]{1,0:T(8,128)(2,1)S(1)} %bitcast.30, bf16[1,1024,2048]{2,1,0:T(8,128)(2,1)} %param.11), kind=kOutput, calls=%fused_computation.4 | convolution fusion | flops 2147483648 | bytes 9437184 | tf_op jit(solution)/shard_map/dot_general | solution.py:8
  42.7 9.2 %fusion.11 = bf16[512,1024]{1,0:T(8,128)(2,1)S(1)} fusion(bf16[1,2048,1024]{2,1,0:T(8,128)(2,1)} %param.13, f32[512,2048]{1,0:T(8,128)} %fusion.4, bf16[512,1024]{1,0:T(8,128)(2,1)S(1)} %bitcast.31, bf16[1,1024,2048]{2,1,0:T(8,128)(2,1)} %param.12), kind=kOutput, calls=%fused_computation.11 | convolution fusion | flops 4301783040 | bytes 14680064 | tf_op jit(solution)/shard_map/dot_general | solution.py:43
  51.9 0.0 copy-start
  51.9 0.0 copy-start.1
  51.9 2.8 %constant_dynamic-slice_fusion = (bf16[32,1,1024]{2,1,0:T(2,128)(2,1)S(1)}, bf16[32,1,1024]{2,1,0:T(2,128)(2,1)S(1)}, bf16[32,1,1024]{2,1,0:T(2,128)(2,1)S(1)}, ...) fusion(bf16[32,16,1024]{2,1,0:T(8,128)(2,1)S(1)} %bitcast.28, ...), kind=kLoop, calls=%fused_computation.29 | loop fusion | bytes 2097216 | tf_op jit(solution)/shard_map/dynamic_slice | solution.py:56
  54.7 0.1 collective-permute-start
  54.8 0.1 collective-permute-start.1
  54.9 2.0 %collective-permute-start.2 = (bf16[32,1,1024]{2,1,0:T(2,128)(2,1)S(1)}, bf16[32,1,1024]{2,1,0:T(2,128)(2,1)S(1)}, u32[]{:S(2)}, u32[]{:S(2)}) collective-permute-start(bf16[32,1,1024]{2,1,0:T(2,128)(2,1)S(1)} %get-tuple-element.17), channel_id=1, source_target_pairs={{0,3},{1,2},{2,1},{3,0},{4,7},{5,6},{6,5},{7,4},{8,11},{9,10},{10,... | collective-permute-start | bytes 196616 | tf_op jit(solution)/shard_map/ppermute | solution.py:58
  56.9 2.5 %collective-permute-start.3 = (bf16[32,1,1024]{2,1,0:T(2,128)(2,1)S(1)}, bf16[32,1,1024]{2,1,0:T(2,128)(2,1)S(1)}, u32[]{:S(2)}, u32[]{:S(2)}) collective-permute-start(bf16[32,1,1024]{2,1,0:T(2,128)(2,1)S(1)} %get-tuple-element.16), channel_id=1, source_target_pairs={{0,4},{1,5},{2,6},{3,7},{4,0},{5,1},{6,2},{7,3},{8,12},{9,13},{10,... | collective-permute-start | bytes 196616 | tf_op jit(solution)/shard_map/ppermute | solution.py:58
  59.4 0.0 collective-permute-start.4
  59.4 0.0 collective-permute-done
  59.4 1.5 %collective-permute-start.5 = (bf16[32,1,1024]{2,1,0:T(2,128)(2,1)S(1)}, bf16[32,1,1024]{2,1,0:T(2,128)(2,1)S(1)}, u32[]{:S(2)}, u32[]{:S(2)}) collective-permute-start(bf16[32,1,1024]{2,1,0:T(2,128)(2,1)S(1)} %get-tuple-element.14), channel_id=1, source_target_pairs={{0,6},{1,7},{2,4},{3,5},{4,2},{5,3},{6,0},{7,1},{8,14},{9,15},{10,... | collective-permute-start | bytes 196616 | tf_op jit(solution)/shard_map/ppermute | solution.py:58
  60.9 0.0 collective-permute-done.1
  61.0 3.2 %collective-permute-start.6 = (bf16[32,1,1024]{2,1,0:T(2,128)(2,1)S(1)}, bf16[32,1,1024]{2,1,0:T(2,128)(2,1)S(1)}, u32[]{:S(2)}, u32[]{:S(2)}) collective-permute-start(bf16[32,1,1024]{2,1,0:T(2,128)(2,1)S(1)} %get-tuple-element.13), channel_id=1, source_target_pairs={{0,7},{1,6},{2,5},{3,4},{4,3},{5,2},{6,1},{7,0},{8,15},{9,14},{10,... | collective-permute-start | bytes 196616 | tf_op jit(solution)/shard_map/ppermute | solution.py:58
  64.1 0.0 collective-permute-done.2
  64.1 1.9 %collective-permute-start.7 = (bf16[32,1,1024]{2,1,0:T(2,128)(2,1)S(1)}, bf16[32,1,1024]{2,1,0:T(2,128)(2,1)S(1)}, u32[]{:S(2)}, u32[]{:S(2)}) collective-permute-start(bf16[32,1,1024]{2,1,0:T(2,128)(2,1)S(1)} %get-tuple-element.12), channel_id=1, source_target_pairs={{0,8},{1,9},{2,10},{3,11},{4,12},{5,13},{6,14},{7,15},{8,0},{9,1},... | collective-permute-start | bytes 196616 | tf_op jit(solution)/shard_map/ppermute | solution.py:58
  66.0 0.0 collective-permute-done.3
  66.0 0.0 collective-permute-start.8
  66.1 0.2 collective-permute-done.4
  66.3 3.3 %collective-permute-start.9 = (bf16[32,1,1024]{2,1,0:T(2,128)(2,1)S(1)}, bf16[32,1,1024]{2,1,0:T(2,128)(2,1)S(1)}, u32[]{:S(2)}, u32[]{:S(2)}) collective-permute-start(bf16[32,1,1024]{2,1,0:T(2,128)(2,1)S(1)} %get-tuple-element.10), channel_id=1, source_target_pairs={{0,10},{1,11},{2,8},{3,9},{4,14},{5,15},{6,12},{7,13},{8,2},{9,3},... | collective-permute-start | bytes 196616 | tf_op jit(solution)/shard_map/ppermute | solution.py:58
  69.6 0.1 copy.18
  69.7 5.3 %collective-permute-done.5 = bf16[32,1,1024]{2,1,0:T(2,128)(2,1)S(1)} collective-permute-done((bf16[32,1,1024]{2,1,0:T(2,128)(2,1)S(1)}, bf16[32,1,1024]{2,1,0:T(2,128)(2,1)S(1)}, u32[]{:S(2)}, u32[]{:S(2)}) %collective-permute-start.5) | collective-permute-done | bytes 65568 | tf_op jit(solution)/shard_map/ppermute | solution.py:58
  75.0 0.5 collective-permute-start.10
  75.5 2.3 %collective-permute-done.6 = bf16[32,1,1024]{2,1,0:T(2,128)(2,1)S(1)} collective-permute-done((bf16[32,1,1024]{2,1,0:T(2,128)(2,1)S(1)}, bf16[32,1,1024]{2,1,0:T(2,128)(2,1)S(1)}, u32[]{:S(2)}, u32[]{:S(2)}) %collective-permute-start.6) | collective-permute-done | bytes 65568 | tf_op jit(solution)/shard_map/ppermute | solution.py:58
  77.8 1.8 %collective-permute-start.11 = (bf16[32,1,1024]{2,1,0:T(2,128)(2,1)S(1)}, bf16[32,1,1024]{2,1,0:T(2,128)(2,1)}, u32[]{:S(2)}, u32[]{:S(2)}) collective-permute-start(bf16[32,1,1024]{2,1,0:T(2,128)(2,1)S(1)} %get-tuple-element.8), channel_id=1, source_target_pairs={{0,12},{1,13},{2,14},{3,15},{4,8},{5,9},{6,10},{7,11},{8,4},{9,5},... | collective-permute-start | bytes 196616 | tf_op jit(solution)/shard_map/ppermute | solution.py:58
  79.6 0.0 collective-permute-done.7
  79.6 2.0 %collective-permute-start.12 = (bf16[32,1,1024]{2,1,0:T(2,128)(2,1)S(1)}, bf16[32,1,1024]{2,1,0:T(2,128)(2,1)}, u32[]{:S(2)}, u32[]{:S(2)}) collective-permute-start(bf16[32,1,1024]{2,1,0:T(2,128)(2,1)S(1)} %get-tuple-element.7), channel_id=1, source_target_pairs={{0,13},{1,12},{2,15},{3,14},{4,9},{5,8},{6,11},{7,10},{8,5},{9,4},... | collective-permute-start | bytes 196616 | tf_op jit(solution)/shard_map/ppermute | solution.py:58
  81.6 8.3 %collective-permute-done.8 = bf16[32,1,1024]{2,1,0:T(2,128)(2,1)S(1)} collective-permute-done((bf16[32,1,1024]{2,1,0:T(2,128)(2,1)S(1)}, bf16[32,1,1024]{2,1,0:T(2,128)(2,1)S(1)}, u32[]{:S(2)}, u32[]{:S(2)}) %collective-permute-start.8) | collective-permute-done | bytes 65568 | tf_op jit(solution)/shard_map/ppermute | solution.py:58
  89.9 2.5 %collective-permute-start.13 = (bf16[32,1,1024]{2,1,0:T(2,128)(2,1)S(1)}, bf16[32,1,1024]{2,1,0:T(2,128)(2,1)}, u32[]{:S(2)}, u32[]{:S(2)}) collective-permute-start(bf16[32,1,1024]{2,1,0:T(2,128)(2,1)S(1)} %get-tuple-element.6), channel_id=1, source_target_pairs={{0,14},{1,15},{2,12},{3,13},{4,10},{5,11},{6,8},{7,9},{8,6},{9,7},... | collective-permute-start | bytes 196616 | tf_op jit(solution)/shard_map/ppermute | solution.py:58
  92.5 1.3 %collective-permute-done.9 = bf16[32,1,1024]{2,1,0:T(2,128)(2,1)S(1)} collective-permute-done((bf16[32,1,1024]{2,1,0:T(2,128)(2,1)S(1)}, bf16[32,1,1024]{2,1,0:T(2,128)(2,1)S(1)}, u32[]{:S(2)}, u32[]{:S(2)}) %collective-permute-start.9) | collective-permute-done | bytes 65568 | tf_op jit(solution)/shard_map/ppermute | solution.py:58
  93.8 4.4 %collective-permute-start.14 = (bf16[32,1,1024]{2,1,0:T(2,128)(2,1)S(1)}, bf16[32,1,1024]{2,1,0:T(2,128)(2,1)S(1)}, u32[]{:S(2)}, u32[]{:S(2)}) collective-permute-start(bf16[32,1,1024]{2,1,0:T(2,128)(2,1)S(1)} %get-tuple-element.5), channel_id=1, source_target_pairs={{0,15},{1,14},{2,13},{3,12},{4,11},{5,10},{6,9},{7,8},{8,7},{9,6},... | collective-permute-start | bytes 196616 | tf_op jit(solution)/shard_map/ppermute | solution.py:58
  98.2 0.6 select_reduce_fusion
  98.8 0.1 broadcast_in_dim.45
  98.9 1.0 dynamic_update_slice.48
  99.9 1.0 dynamic_update_slice.49
  101.0 1.0 dynamic_update_slice.50
  102.0 1.0 dynamic_update_slice.51
  103.0 1.0 dynamic_update_slice.52
  104.0 1.0 dynamic_update_slice.53
  105.0 1.0 dynamic_update_slice.54
  106.0 1.0 dynamic_update_slice.55
  107.0 1.0 dynamic_update_slice.56
  108.0 1.0 dynamic_update_slice.57
  109.0 1.0 dynamic_update_slice.58
  110.1 0.0 collective-permute-done.10
  110.1 2.2 %dynamic_update_slice.59 = bf16[32,16,1024]{2,1,0:T(8,128)(2,1)S(1)} dynamic-update-slice(bf16[32,16,1024]{2,1,0:T(8,128)(2,1)S(1)} %dynamic_update_slice.58, bf16[32,1,1024]{2,1,0:T(2,128)(2,1)} %collective-permute-done.10, s32[]{:T(128)} %constant.26.clone.1, s32[]{:T(128)S(6)} %select_n.94, s32[]{:T(128)} %constant.26.clone.1) | dynamic-update-slice | bytes 131076 | tf_op jit(solution)/shard_map/dynamic_update_slice | solution.py:59
  112.3 0.0 collective-permute-done.11
  112.3 2.2 %dynamic_update_slice.60 = bf16[32,16,1024]{2,1,0:T(8,128)(2,1)S(1)} dynamic-update-slice(bf16[32,16,1024]{2,1,0:T(8,128)(2,1)S(1)} %dynamic_update_slice.59, bf16[32,1,1024]{2,1,0:T(2,128)(2,1)} %collective-permute-done.11, s32[]{:T(128)} %constant.26.clone.1, s32[]{:T(128)S(6)} %select_n.95, s32[]{:T(128)} %constant.26.clone.1) | dynamic-update-slice | bytes 131076 | tf_op jit(solution)/shard_map/dynamic_update_slice | solution.py:59
  114.6 0.0 collective-permute-done.12
  114.6 2.2 %dynamic_update_slice.61 = bf16[32,16,1024]{2,1,0:T(8,128)(2,1)S(1)} dynamic-update-slice(bf16[32,16,1024]{2,1,0:T(8,128)(2,1)S(1)} %dynamic_update_slice.60, bf16[32,1,1024]{2,1,0:T(2,128)(2,1)} %collective-permute-done.12, s32[]{:T(128)} %constant.26.clone.1, s32[]{:T(128)S(6)} %select_n.96, s32[]{:T(128)} %constant.26.clone.1) | dynamic-update-slice | bytes 131076 | tf_op jit(solution)/shard_map/dynamic_update_slice | solution.py:59
  116.9 2.2 %dynamic_update_slice.62 = bf16[32,16,1024]{2,1,0:T(8,128)(2,1)S(1)} dynamic-update-slice(bf16[32,16,1024]{2,1,0:T(8,128)(2,1)S(1)} %dynamic_update_slice.61, bf16[32,1,1024]{2,1,0:T(2,128)(2,1)} %collective-permute-done.13, s32[]{:T(128)} %constant.26.clone.1, s32[]{:T(128)S(6)} %select_n.97, s32[]{:T(128)} %constant.26.clone.1) | dynamic-update-slice | bytes 131076 | tf_op jit(solution)/shard_map/dynamic_update_slice | solution.py:59
  119.1 1.0 dynamic_update_slice.63
  120.1 0.3 fusion.23
  120.4 1.0 fusion.16
  (8 shorter events, 0.0 us)
Async XLA Ops:
  5.5 30.2 %all-to-all-start = ((bf16[32,16,1024]{2,0,1:T(8,128)(2,1)}), bf16[32,16,1024]{2,0,1:T(8,128)(2,1)S(1)}, u32[]{:S(2)}, u32[]{:S(2)}) async-start(bf16[32,16,1024]{2,0,1:T(8,128)(2,1)} %copy.19), calls=%async_computation | async-start | bytes 2097152 | tf_op jit(solution)/shard_map/all_to_all | solution.py:41
  51.9 17.7 %copy-start = (s32[64,6]{0,1:T(8,128)S(1)}, s32[64,6]{0,1:T(8,128)}, u32[]{:S(2)}) copy-start(s32[64,6]{0,1:T(8,128)} %param.9) | copy-start | bytes 4612
  51.9 17.7 %copy-start.1 = (f32[64,6]{0,1:T(8,128)S(1)}, f32[64,6]{0,1:T(8,128)}, u32[]{:S(2)}) copy-start(f32[64,6]{0,1:T(8,128)} %param.10) | copy-start | bytes 4612
  54.7 4.7 %collective-permute-start = (bf16[32,1,1024]{2,1,0:T(2,128)(2,1)S(1)}, bf16[32,1,1024]{2,1,0:T(2,128)(2,1)S(1)}, u32[]{:S(2)}, u32[]{:S(2)}) collective-permute-start(bf16[32,1,1024]{2,1,0:T(2,128)(2,1)S(1)} %get-tuple-element.19), channel_id=1, source_target_pairs={{0,1},{1,0},{2,3},{3,2},{4,5},{5,4},{6,7},{7,6},{8,9},{9,8},{10,11... | collective-permute-start | bytes 196616 | tf_op jit(solution)/shard_map/ppermute | solution.py:58
  54.8 6.2 %collective-permute-start.1 = (bf16[32,1,1024]{2,1,0:T(2,128)(2,1)S(1)}, bf16[32,1,1024]{2,1,0:T(2,128)(2,1)S(1)}, u32[]{:S(2)}, u32[]{:S(2)}) collective-permute-start(bf16[32,1,1024]{2,1,0:T(2,128)(2,1)S(1)} %get-tuple-element.18), channel_id=1, source_target_pairs={{0,2},{1,3},{2,0},{3,1},{4,6},{5,7},{6,4},{7,5},{8,10},{9,11},{10,... | collective-permute-start | bytes 196616 | tf_op jit(solution)/shard_map/ppermute | solution.py:58
  54.9 9.3 %collective-permute-start.2 = (bf16[32,1,1024]{2,1,0:T(2,128)(2,1)S(1)}, bf16[32,1,1024]{2,1,0:T(2,128)(2,1)S(1)}, u32[]{:S(2)}, u32[]{:S(2)}) collective-permute-start(bf16[32,1,1024]{2,1,0:T(2,128)(2,1)S(1)} %get-tuple-element.17), channel_id=1, source_target_pairs={{0,3},{1,2},{2,1},{3,0},{4,7},{5,6},{6,5},{7,4},{8,11},{9,10},{10,... | collective-permute-start | bytes 196616 | tf_op jit(solution)/shard_map/ppermute | solution.py:58
  56.9 9.1 %collective-permute-start.3 = (bf16[32,1,1024]{2,1,0:T(2,128)(2,1)S(1)}, bf16[32,1,1024]{2,1,0:T(2,128)(2,1)S(1)}, u32[]{:S(2)}, u32[]{:S(2)}) collective-permute-start(bf16[32,1,1024]{2,1,0:T(2,128)(2,1)S(1)} %get-tuple-element.16), channel_id=1, source_target_pairs={{0,4},{1,5},{2,6},{3,7},{4,0},{5,1},{6,2},{7,3},{8,12},{9,13},{10,... | collective-permute-start | bytes 196616 | tf_op jit(solution)/shard_map/ppermute | solution.py:58
  59.4 6.8 %collective-permute-start.4 = (bf16[32,1,1024]{2,1,0:T(2,128)(2,1)S(1)}, bf16[32,1,1024]{2,1,0:T(2,128)(2,1)S(1)}, u32[]{:S(2)}, u32[]{:S(2)}) collective-permute-start(bf16[32,1,1024]{2,1,0:T(2,128)(2,1)S(1)} %get-tuple-element.15), channel_id=1, source_target_pairs={{0,5},{1,4},{2,7},{3,6},{4,1},{5,0},{6,3},{7,2},{8,13},{9,12},{10,... | collective-permute-start | bytes 196616 | tf_op jit(solution)/shard_map/ppermute | solution.py:58
  59.4 15.6 %collective-permute-start.5 = (bf16[32,1,1024]{2,1,0:T(2,128)(2,1)S(1)}, bf16[32,1,1024]{2,1,0:T(2,128)(2,1)S(1)}, u32[]{:S(2)}, u32[]{:S(2)}) collective-permute-start(bf16[32,1,1024]{2,1,0:T(2,128)(2,1)S(1)} %get-tuple-element.14), channel_id=1, source_target_pairs={{0,6},{1,7},{2,4},{3,5},{4,2},{5,3},{6,0},{7,1},{8,14},{9,15},{10,... | collective-permute-start | bytes 196616 | tf_op jit(solution)/shard_map/ppermute | solution.py:58
  61.0 16.8 %collective-permute-start.6 = (bf16[32,1,1024]{2,1,0:T(2,128)(2,1)S(1)}, bf16[32,1,1024]{2,1,0:T(2,128)(2,1)S(1)}, u32[]{:S(2)}, u32[]{:S(2)}) collective-permute-start(bf16[32,1,1024]{2,1,0:T(2,128)(2,1)S(1)} %get-tuple-element.13), channel_id=1, source_target_pairs={{0,7},{1,6},{2,5},{3,4},{4,3},{5,2},{6,1},{7,0},{8,15},{9,14},{10,... | collective-permute-start | bytes 196616 | tf_op jit(solution)/shard_map/ppermute | solution.py:58
  64.1 15.5 %collective-permute-start.7 = (bf16[32,1,1024]{2,1,0:T(2,128)(2,1)S(1)}, bf16[32,1,1024]{2,1,0:T(2,128)(2,1)S(1)}, u32[]{:S(2)}, u32[]{:S(2)}) collective-permute-start(bf16[32,1,1024]{2,1,0:T(2,128)(2,1)S(1)} %get-tuple-element.12), channel_id=1, source_target_pairs={{0,8},{1,9},{2,10},{3,11},{4,12},{5,13},{6,14},{7,15},{8,0},{9,1},... | collective-permute-start | bytes 196616 | tf_op jit(solution)/shard_map/ppermute | solution.py:58
  66.0 23.9 %collective-permute-start.8 = (bf16[32,1,1024]{2,1,0:T(2,128)(2,1)S(1)}, bf16[32,1,1024]{2,1,0:T(2,128)(2,1)S(1)}, u32[]{:S(2)}, u32[]{:S(2)}) collective-permute-start(bf16[32,1,1024]{2,1,0:T(2,128)(2,1)S(1)} %get-tuple-element.11), channel_id=1, source_target_pairs={{0,9},{1,8},{2,11},{3,10},{4,13},{5,12},{6,15},{7,14},{8,1},{9,0},... | collective-permute-start | bytes 196616 | tf_op jit(solution)/shard_map/ppermute | solution.py:58
  66.3 27.5 %collective-permute-start.9 = (bf16[32,1,1024]{2,1,0:T(2,128)(2,1)S(1)}, bf16[32,1,1024]{2,1,0:T(2,128)(2,1)S(1)}, u32[]{:S(2)}, u32[]{:S(2)}) collective-permute-start(bf16[32,1,1024]{2,1,0:T(2,128)(2,1)S(1)} %get-tuple-element.10), channel_id=1, source_target_pairs={{0,10},{1,11},{2,8},{3,9},{4,14},{5,15},{6,12},{7,13},{8,2},{9,3},... | collective-permute-start | bytes 196616 | tf_op jit(solution)/shard_map/ppermute | solution.py:58
  75.0 35.1 %collective-permute-start.10 = (bf16[32,1,1024]{2,1,0:T(2,128)(2,1)S(1)}, bf16[32,1,1024]{2,1,0:T(2,128)(2,1)}, u32[]{:S(2)}, u32[]{:S(2)}) collective-permute-start(bf16[32,1,1024]{2,1,0:T(2,128)(2,1)S(1)} %get-tuple-element.9), channel_id=1, source_target_pairs={{0,11},{1,10},{2,9},{3,8},{4,15},{5,14},{6,13},{7,12},{8,3},{9,2},... | collective-permute-start | bytes 196616 | tf_op jit(solution)/shard_map/ppermute | solution.py:58
  77.8 34.6 %collective-permute-start.11 = (bf16[32,1,1024]{2,1,0:T(2,128)(2,1)S(1)}, bf16[32,1,1024]{2,1,0:T(2,128)(2,1)}, u32[]{:S(2)}, u32[]{:S(2)}) collective-permute-start(bf16[32,1,1024]{2,1,0:T(2,128)(2,1)S(1)} %get-tuple-element.8), channel_id=1, source_target_pairs={{0,12},{1,13},{2,14},{3,15},{4,8},{5,9},{6,10},{7,11},{8,4},{9,5},... | collective-permute-start | bytes 196616 | tf_op jit(solution)/shard_map/ppermute | solution.py:58
  79.6 35.0 %collective-permute-start.12 = (bf16[32,1,1024]{2,1,0:T(2,128)(2,1)S(1)}, bf16[32,1,1024]{2,1,0:T(2,128)(2,1)}, u32[]{:S(2)}, u32[]{:S(2)}) collective-permute-start(bf16[32,1,1024]{2,1,0:T(2,128)(2,1)S(1)} %get-tuple-element.7), channel_id=1, source_target_pairs={{0,13},{1,12},{2,15},{3,14},{4,9},{5,8},{6,11},{7,10},{8,5},{9,4},... | collective-permute-start | bytes 196616 | tf_op jit(solution)/shard_map/ppermute | solution.py:58
  89.9 26.9 %collective-permute-start.13 = (bf16[32,1,1024]{2,1,0:T(2,128)(2,1)S(1)}, bf16[32,1,1024]{2,1,0:T(2,128)(2,1)}, u32[]{:S(2)}, u32[]{:S(2)}) collective-permute-start(bf16[32,1,1024]{2,1,0:T(2,128)(2,1)S(1)} %get-tuple-element.6), channel_id=1, source_target_pairs={{0,14},{1,15},{2,12},{3,13},{4,10},{5,11},{6,8},{7,9},{8,6},{9,7},... | collective-permute-start | bytes 196616 | tf_op jit(solution)/shard_map/ppermute | solution.py:58
  93.8 25.4 %collective-permute-start.14 = (bf16[32,1,1024]{2,1,0:T(2,128)(2,1)S(1)}, bf16[32,1,1024]{2,1,0:T(2,128)(2,1)S(1)}, u32[]{:S(2)}, u32[]{:S(2)}) collective-permute-start(bf16[32,1,1024]{2,1,0:T(2,128)(2,1)S(1)} %get-tuple-element.5), channel_id=1, source_target_pairs={{0,15},{1,14},{2,13},{3,12},{4,11},{5,10},{6,9},{7,8},{8,7},{9,6},... | collective-permute-start | bytes 196616 | tf_op jit(solution)/shard_map/ppermute | solution.py:58
